TPU v7x, 32 devices: a whole 2x2x4 slice. The times are simulated.
32 devices in a mesh: kv: 4 (over y, x), tp: 8 (over z, core).
Axes of the slice: x: 2, y: 2, z: 4, core: 2. Of those that a mesh axis runs over, the one named last changes fastest.
Arguments:
- hidden_in: bfloat16 [16, 4096], P('kv', 'tp'), may hold values from -12 to 12
- mixer_gain: float32 [4096], P('tp'), may hold values from 0.1 to 1.9
- query_weight: bfloat16 [4096, 4096], P('tp', 'kv'), may hold values from -0.09375 to 0.09375
- key_weight: bfloat16 [4096, 4096], P('tp', 'kv'), may hold values from -0.09375 to 0.09375
- value_weight: bfloat16 [4096, 8192], P('tp', 'kv'), may hold values from -0.09375 to 0.09375
- gate_weight: bfloat16 [4096, 8192], P('tp', 'kv'), may hold values from -0.09375 to 0.09375
- decay_rate: float32 [16], P('kv'), may hold values from 0.0005 to 0.15
- prior_state: float32 [16, 16, 256, 512], P('tp', 'kv'), may hold values from -2.5 to 2.5
- key_block: bfloat16 [16, 16, 128, 256], P('tp', 'kv'), may hold values from -1 to 1
- value_block: bfloat16 [16, 16, 128, 512], P('tp', 'kv'), may hold values from -6 to 6
- lengths: int32 [16], P('tp'), may hold values from 1 to 16384, 65536 in all
- group_gain: float32 [8192], P('kv'), may hold values from 0.1 to 1.9
- output_weight: bfloat16 [8192, 4096], P('kv', 'tp'), may hold values from -0.0625 to 0.0625
- channel_gain: float32 [4096], P('tp'), may hold values from 0.1 to 1.9
- hidden_gate: bfloat16 [4096, 11264], P('tp', 'kv'), may hold values from -0.09375 to 0.09375
- hidden_up: bfloat16 [4096, 11264], P('tp', 'kv'), may hold values from -0.09375 to 0.09375
- hidden_down: bfloat16 [11264, 4096], P('kv', 'tp'), may hold values from -0.0546875 to 0.0546875
Outputs:
- layer_out: bfloat16 [16, 4096], P('kv', 'tp')
Inputs may be any that keep to these rules, and one draw needn't show every extreme that they name: Sequence s has lengths[s] earlier positions; slots 0 to (lengths[s] mod 128) - 1 of key_block and value_block hold the turned, scaled keys and the values of its positions from 128 * floor(lengths[s] / 128) on, prior_state holds the state of the positions before them, and the other slots take no part.
All inputs are finite; a program needn't handle non-finite values. No bound on the sum of `lengths` on one device may be relied on, other than what follows from the above.
Results may differ from a plain program's by a relative error of at most 0.029.
Values may be sent and summed in bfloat16 or wider, within the bound.
A program may use at most 64 MiB of HBM per device.

v0:
```python
import jax
import jax.numpy as jnp
from jax import lax
from jax.sharding import PartitionSpec as P

D = 4096
epsilon = 1e-06


def as_sent(value):
    return jax.tree.map(lambda a: a.astype(jnp.bfloat16) if a.dtype == jnp.float32 else a, value)


def rotate(vectors, position):
    half_dim = vectors.shape[-1] // 2
    inverse = 10000.0 ** (-jnp.arange(half_dim, dtype=jnp.float32) / half_dim)
    angles = position.astype(jnp.float32)[:, None, None] * inverse
    cosine_part = jnp.cos(angles)
    sine_part = jnp.sin(angles)
    front_half = vectors[..., :half_dim]
    back_half = vectors[..., half_dim:]
    return jnp.concatenate(
        [
            front_half * cosine_part - back_half * sine_part,
            front_half * sine_part + back_half * cosine_part,
        ],
        axis=-1,
    )


def retain(
    queries,
    keys_new,
    values_new,
    gates,
    decay_rate,
    prior_state,
    key_block,
    value_block,
    lengths,
    group_gain,
):
    batch_rows = queries.shape[0]
    heads_here = decay_rate.shape[0]
    key_width = prior_state.shape[2]
    value_width = prior_state.shape[3]
    block_len = key_block.shape[2]
    rotated = rotate(
        queries.astype(jnp.float32).reshape(batch_rows, heads_here, key_width), lengths
    ).astype(jnp.bfloat16)
    fresh_keys = rotate(
        keys_new.astype(jnp.float32).reshape(batch_rows, heads_here, key_width), lengths
    ) * key_width ** (-0.5)
    fresh_values = values_new.astype(jnp.float32).reshape(batch_rows, heads_here, value_width)
    filled = lengths % block_len
    slots = jnp.arange(block_len, dtype=jnp.int32)
    distance = (filled[:, None] - slots[None, :]).astype(jnp.float32)
    live_slots = (slots[None, :] < filled[:, None])[:, None, :]
    weighting = jnp.where(
        live_slots, jnp.exp(-decay_rate[None, :, None] * distance[:, None, :]), jnp.float32(0.0)
    )
    scores = jnp.einsum("shk,shjk->shj", rotated, key_block, preferred_element_type=jnp.float32)
    block_weights = (scores * weighting).astype(jnp.bfloat16)
    block_term = jnp.einsum(
        "shj,shjv->shv", block_weights, value_block, preferred_element_type=jnp.float32
    )
    rotated_wide = rotated.astype(jnp.float32)
    own_term = jnp.sum(rotated_wide * fresh_keys, axis=-1, keepdims=True) * fresh_values
    carried = jnp.exp(-decay_rate[None, :, None] * (filled[:, None, None] + 1).astype(jnp.float32))
    state_term = carried * jnp.einsum(
        "shk,shkv->shv", rotated_wide, prior_state, precision=lax.Precision.HIGHEST
    )
    retained = own_term + block_term + state_term
    centre = jnp.mean(retained, axis=-1, keepdims=True)
    spread = jnp.mean(jnp.square(retained - centre), axis=-1, keepdims=True)
    normed = (retained - centre) * lax.rsqrt(spread + epsilon)
    gated = (
        jax.nn.silu(gates.astype(jnp.float32)).reshape(batch_rows, heads_here, value_width)
        * normed
        * group_gain.reshape(heads_here, value_width)
    )
    return gated.astype(jnp.bfloat16).reshape(batch_rows, heads_here * value_width)


def local(
    hidden_in,
    mixer_gain,
    query_weight,
    key_weight,
    value_weight,
    gate_weight,
    decay_rate,
    prior_state,
    key_block,
    value_block,
    lengths,
    group_gain,
    output_weight,
    channel_gain,
    hidden_gate,
    hidden_up,
    hidden_down,
):
    local_seqs = lengths.shape[0]
    group_count = lax.axis_size("tp")
    first_row = lax.axis_index("tp") * local_seqs
    stream = hidden_in.astype(jnp.float32)
    scaled_in = (stream * mixer_gain).astype(jnp.bfloat16)
    own_squares = jnp.sum(stream * stream, axis=1)
    own_squares = lax.psum(own_squares, "tp")
    all_rows, all_squares = (
        lax.all_gather(scaled_in, "kv", axis=0, tiled=True),
        lax.all_gather(own_squares.astype(jnp.bfloat16), "kv", axis=0, tiled=True).astype(
            own_squares.dtype
        ),
    )
    weights_in = (query_weight, key_weight, value_weight, gate_weight)
    shaped_rows = all_rows.reshape(group_count, local_seqs, all_rows.shape[1])
    half_seqs = local_seqs // 2
    pieces = []
    for portion in range(2):
        rows_part = shaped_rows[:, portion * half_seqs : (portion + 1) * half_seqs].reshape(
            group_count * half_seqs, all_rows.shape[1]
        )
        terms = tuple(
            (
                jnp.dot(rows_part, matrix, preferred_element_type=jnp.float32)
                for matrix in weights_in
            )
        )
        pieces.append(
            jax.tree.map(
                lambda part: part.astype(jnp.float32),
                lax.psum_scatter(as_sent(terms), "tp", scatter_dimension=0, tiled=True),
            )
        )
    summed = tuple(
        (
            jnp.concatenate([pieces[0][member], pieces[1][member]], axis=0)
            for member in range(len(pieces[0]))
        )
    )
    row_squares = lax.dynamic_slice_in_dim(all_squares, first_row, local_seqs, 0)
    first_scale = lax.rsqrt(row_squares / D + epsilon)[:, None]
    queries = (first_scale * summed[0]).astype(jnp.bfloat16)
    keys_new = (first_scale * summed[1]).astype(jnp.bfloat16)
    values_new = (first_scale * summed[2]).astype(jnp.bfloat16)
    gates = (first_scale * summed[3]).astype(jnp.bfloat16)
    mixed = retain(
        queries,
        keys_new,
        values_new,
        gates,
        decay_rate,
        prior_state,
        key_block,
        value_block,
        lengths,
        group_gain,
    )
    head_terms = jnp.dot(
        lax.all_gather(mixed, "tp", axis=0, tiled=True),
        output_weight,
        preferred_element_type=jnp.float32,
    )
    mixer_out = lax.psum_scatter(
        head_terms.astype(jnp.bfloat16), "kv", scatter_dimension=0, tiled=True
    ).astype(jnp.float32)
    middle = stream + mixer_out
    scaled_mid = (middle * channel_gain).astype(jnp.bfloat16)
    middle_squares = jnp.sum(middle * middle, axis=1)
    middle_squares = lax.psum(middle_squares, "tp")
    middle_rows, middle_all = (
        lax.all_gather(scaled_mid, "kv", axis=0, tiled=True),
        lax.all_gather(middle_squares.astype(jnp.bfloat16), "kv", axis=0, tiled=True).astype(
            middle_squares.dtype
        ),
    )
    channel_terms = (
        jnp.dot(middle_rows, hidden_gate, preferred_element_type=jnp.float32),
        jnp.dot(middle_rows, hidden_up, preferred_element_type=jnp.float32),
    )
    channel_summed = (
        lax.psum_scatter(
            channel_terms[0].astype(jnp.bfloat16), "tp", scatter_dimension=0, tiled=True
        ).astype(jnp.float32),
        lax.psum_scatter(
            channel_terms[1].astype(jnp.bfloat16), "tp", scatter_dimension=0, tiled=True
        ).astype(jnp.float32),
    )
    middle_row_squares = lax.dynamic_slice_in_dim(middle_all, first_row, local_seqs, 0)
    second_scale = lax.rsqrt(middle_row_squares / D + epsilon)[:, None]
    gate_part = second_scale * channel_summed[0]
    up_part = second_scale * channel_summed[1]
    activated = (jax.nn.silu(gate_part) * up_part).astype(jnp.bfloat16)
    unit_terms = jnp.dot(
        lax.all_gather(activated, "tp", axis=0, tiled=True),
        hidden_down,
        preferred_element_type=jnp.float32,
    )
    channel_out = lax.psum_scatter(
        unit_terms.astype(jnp.bfloat16), "kv", scatter_dimension=0, tiled=True
    ).astype(jnp.float32)
    return (middle + channel_out).astype(jnp.bfloat16)


def solution(mesh):
    in_specs = (
        P("kv", "tp"),
        P("tp"),
        P("tp", "kv"),
        P("tp", "kv"),
        P("tp", "kv"),
        P("tp", "kv"),
        P("kv"),
        P("tp", "kv", None, None),
        P("tp", "kv", None, None),
        P("tp", "kv", None, None),
        P("tp"),
        P("kv"),
        P("kv", "tp"),
        P("tp"),
        P("tp", "kv"),
        P("tp", "kv"),
        P("kv", "tp"),
    )
    out_specs = P("kv", "tp")
    return jax.shard_map(local, mesh=mesh, in_specs=in_specs, out_specs=out_specs, check_vma=False)
```

profile of v0, /device:TPU:0, one launch (start us, length us, event | category | flops | bytes accessed | tf_op | source)
XLA Modules:
  0.0 253.7 jit_solution(16599473605607127361)
XLA Ops:
  7.5 9.7 %all-gather = bf16[4,4,512]{2,1,0:T(4,128)(2,1)S(1)} all-gather(bf16[1,4,512]{2,1,0:T(4,128)(2,1)S(1)} %get-tuple-element.28), channel_id=1, replica_groups=mesh['kv'=4,'tp'=8] {'kv'}, dimensions={0}, use_global_device_ids=true | all-gather | bytes 20480 | tf_op jit(solution)/shard_map/all_gather | solution.py:112
  17.3 2.7 %convolution_convert_fusion.2 = bf16[8,2048]{1,0:T(8,128)(2,1)} fusion(bf16[512,2048]{1,0:T(8,128)(2,1)} %param.21, bf16[8,1,512]{2,0,1:T(8,128)(2,1)S(1)} %copy.26), kind=kOutput, calls=%fused_computation.2 | convolution fusion | flops 16793600 | bytes 2138112 | tf_op jit(solution)/shard_map/dot_general | solution.py:127
  20.0 1.0 convolution_convert_fusion.3
  26.7 14.6 %psum.14 = bf16[4]{0:T(256)(128)(2,1)S(1)} all-reduce(f32[4]{0:T(128)S(1)} %get-tuple-element.27), channel_id=1, replica_groups=mesh['kv'=4,'tp'=8] {'tp'}, use_global_device_ids=true, to_apply=%region_1.0 | all-reduce | flops 4 | bytes 24 | tf_op jit(solution)/shard_map/psum | solution.py:110
  43.5 8.9 %all-reduce = bf16[16]{0:T(256)(128)(2,1)S(1)} all-reduce(bf16[16]{0:T(256)(128)(2,1)S(1)} %dynamic-update-slice), channel_id=1, replica_groups=mesh['kv'=4,'tp'=8] {'kv'}, use_global_device_ids=true, to_apply=%add | all-reduce | flops 16 | bytes 64
  54.1 29.0 %all-reduce.19.cloned.1.call-done = (bf16[8,1024]{1,0:T(8,128)(2,1)}, bf16[8,1024]{1,0:T(8,128)(2,1)}, bf16[8,2048]{1,0:T(8,128)(2,1)}, bf16[8,2048]{1,0:T(8,128...) async-done(((bf16[8,1024]{1,0:T(8,128)(2,1)}, bf16[8,1024]{1,0:T(8,128)(2,1)}, ...) | async-done | bytes 196624
  83.0 1.4 dynamic-slice_reduce_fusion.6
  84.5 1.4 dynamic-slice_reduce_fusion.4
  86.3 3.6 %fusion.19 = f32[2,4,1,512]{3,2,1,0:T(1,128)S(1)} fusion(f32[2,4,256,512]{3,2,1,0:T(8,128)} %param.24, bf16[2,4,256,1]{2,1,0,3:T(4,128)(2,1)S(1)} %fusion.30), kind=kOutput, calls=%fused_computation.53 | convolution fusion | flops 12582912 | bytes 4214784 | tf_op jit(solution)/shard_map/shk,shkv->shv/dot_general | solution.py:70
  89.9 1.5 dynamic-slice_reduce_fusion
  91.6 1.5 fusion.27
  93.4 1.5 dynamic-slice_reduce_fusion.2
  95.1 14.0 %all-gather.1 = bf16[8,2,2048]{2,1,0:T(2,128)(2,1)S(1)} all-gather(bf16[1,2,2048]{2,1,0:T(2,128)(2,1)S(1)} %reshape.210), channel_id=1, replica_groups=mesh['kv'=4,'tp'=8] {'tp'}, dimensions={0}, use_global_device_ids=true | all-gather | bytes 73728 | tf_op jit(solution)/shard_map/all_gather | solution.py:162
  109.1 2.0 convolution_convert_fusion.7
  111.0 16.0 %all-reduce.10 = bf16[16,512]{1,0:T(8,128)(2,1)S(1)} all-reduce(bf16[16,512]{1,0:T(8,128)(2,1)S(1)} %convolution_convert_fusion.7), channel_id=10, replica_groups=mesh['kv'=4,'tp'=8] {'kv'}, use_global_device_ids=true, to_apply=%region_13.14.clone | all-reduce | flops 8192 | bytes 32768
  127.2 7.2 %all-gather.2 = bf16[4,4,512]{2,1,0:T(4,128)(2,1)S(1)} all-gather(bf16[1,4,512]{2,1,0:T(4,128)(2,1)S(1)} %get-tuple-element.20), channel_id=1, replica_groups=mesh['kv'=4,'tp'=8] {'kv'}, dimensions={0}, use_global_device_ids=true | all-gather | bytes 20480 | tf_op jit(solution)/shard_map/all_gather | solution.py:174
  134.4 13.6 %psum.15 = bf16[4]{0:T(256)(128)(2,1)S(1)} all-reduce(f32[4]{0:T(128)S(1)} %get-tuple-element.19), channel_id=1, replica_groups=mesh['kv'=4,'tp'=8] {'tp'}, use_global_device_ids=true, to_apply=%region_15.16 | all-reduce | flops 4 | bytes 24 | tf_op jit(solution)/shard_map/psum | solution.py:172
  148.0 1.1 convolution_convert_fusion
  149.3 3.0 %convolution_convert_fusion.1 = bf16[16,2816]{1,0:T(8,128)(2,1)} fusion(bf16[16,512]{1,0:T(8,128)(2,1)S(1)} %reshape.213, bf16[512,2816]{1,0:T(8,128)(2,1)} %param.31), kind=kOutput, calls=%fused_computation.1 | convolution fusion | flops 46182400 | bytes 2990080 | tf_op jit(solution)/shard_map/dot_general | solution.py:180
  152.3 8.9 %all-reduce.1 = bf16[16]{0:T(256)(128)(2,1)S(1)} all-reduce(bf16[16]{0:T(256)(128)(2,1)S(1)} %dynamic-update-slice.1), channel_id=1, replica_groups=mesh['kv'=4,'tp'=8] {'kv'}, use_global_device_ids=true, to_apply=%add.1 | all-reduce | flops 16 | bytes 64
  161.3 51.1 %all-reduce.21.cloned.1.call-done = (bf16[16,2816]{1,0:T(8,128)(2,1)}, bf16[16,2816]{1,0:T(8,128)(2,1)}) async-done(((bf16[16,2816]{1,0:T(8,128)(2,1)}, bf16[16,2816]{1,0:T(8,128)(2,1)}), (bf16[16,2816]{1,0:T(8,128)(2,1)}, bf16[16,2816]{1,0:T(8,128)(2,1)})) %all-reduce.21.cloned.1.call-update) | async-done | bytes 180240
  213.4 14.6 %all-gather.3 = bf16[8,2,2816]{2,1,0:T(2,128)(2,1)S(1)} all-gather(bf16[1,2,2816]{2,1,0:T(2,128)(2,1)S(1)} %fusion.6), channel_id=1, replica_groups=mesh['kv'=4,'tp'=8] {'tp'}, dimensions={0}, use_global_device_ids=true | all-gather | bytes 101376 | tf_op jit(solution)/shard_map/all_gather | solution.py:197
  227.9 2.3 convolution_convert_fusion.6
  230.2 16.0 %all-reduce.13 = bf16[16,512]{1,0:T(8,128)(2,1)S(1)} all-reduce(bf16[16,512]{1,0:T(8,128)(2,1)S(1)} %convolution_convert_fusion.6), channel_id=13, replica_groups=mesh['kv'=4,'tp'=8] {'kv'}, use_global_device_ids=true, to_apply=%region_18.19.clone | all-reduce | flops 8192 | bytes 32768
  (85 shorter events, 11.5 us)
Async XLA Ops:
  6.5 141.5 %copy-start = (bf16[512,2816]{1,0:T(8,128)(2,1)S(1)}, bf16[512,2816]{1,0:T(8,128)(2,1)}, u32[]{:S(2)}) copy-start(bf16[512,2816]{1,0:T(8,128)(2,1)} %param.32) | copy-start | bytes 8650756
  6.5 76.5 %all-reduce.19.cloned.1.call-start = ((), (), s32[]{:S(2)}) async-start(), calls=%async_computation | async-start | bytes 393216
  17.2 2.8 %copy-start.1 = (bf16[512,2048]{1,0:T(8,128)(2,1)S(1)}, bf16[512,2048]{1,0:T(8,128)(2,1)}, u32[]{:S(2)}) copy-start(bf16[512,2048]{1,0:T(8,128)(2,1)} %param.21) | copy-start | bytes 6291460
  17.3 3.7 %copy-start.2 = (bf16[512,2048]{1,0:T(8,128)(2,1)S(1)}, bf16[512,2048]{1,0:T(8,128)(2,1)}, u32[]{:S(2)}) copy-start(bf16[512,2048]{1,0:T(8,128)(2,1)} %param.22) | copy-start | bytes 6291460
  21.0 2.0 copy-start.3
  22.0 2.7 %copy-start.4 = (bf16[512,1024]{1,0:T(8,128)(2,1)S(1)}, bf16[512,1024]{1,0:T(8,128)(2,1)}, u32[]{:S(2)}) copy-start(bf16[512,1024]{1,0:T(8,128)(2,1)} %param.20) | copy-start | bytes 3145732
  23.0 3.5 %copy-start.10 = (s32[2]{0:T(128)S(1)}, s32[2]{0:T(128)}, u32[]{:S(2)}) copy-start(s32[2]{0:T(128)} %param.27) | copy-start | bytes 28
  23.0 18.3 %copy-start.12 = (u32[32]{0:T(128)S(1)}, u32[32]{0:T(128)}, u32[]{:S(2)}) copy-start(u32[32]{0:T(128)} %constant.69) | copy-start | bytes 388
  23.0 18.9 %copy-start.9 = (u32[32]{0:T(128)S(1)}, u32[32]{0:T(128)}, u32[]{:S(2)}) copy-start(u32[32]{0:T(128)} %constant.57) | copy-start | bytes 388
  23.0 29.5 %copy-start.11 = (f32[4]{0:T(128)S(1)}, f32[4]{0:T(128)}, u32[]{:S(2)}) copy-start(f32[4]{0:T(128)} %param.23) | copy-start | bytes 52
  23.0 29.5 %copy-start.7 = (f32[2048]{0:T(1024)S(1)}, f32[2048]{0:T(1024)}, u32[]{:S(2)}) copy-start(f32[2048]{0:T(1024)} %param.28) | copy-start | bytes 24580
  23.9 62.2 %copy-start.5 = (bf16[2,4,128,256]{3,2,1,0:T(8,128)(2,1)S(1)}, bf16[2,4,128,256]{3,2,1,0:T(8,128)(2,1)}, u32[]{:S(2)}) copy-start(bf16[2,4,128,256]{3,2,1,0:T(8,128)(2,1)} %param.25) | copy-start | bytes 1572868
  26.4 186.0 %all-reduce.21.cloned.1.call-start = ((), (), s32[]{:S(2)}) async-start(), calls=%async_computation.1 | async-start | bytes 360448
  89.9 37.1 %copy-start.6 = (bf16[4,512]{1,0:T(4,128)(2,1)S(1)}, bf16[4,512]{1,0:T(4,128)(2,1)}, u32[]{:S(2)}) copy-start(bf16[4,512]{1,0:T(4,128)(2,1)} %param.17) | copy-start | bytes 12292
  89.9 37.1 %copy-start.8 = (f32[512]{0:T(512)S(1)}, f32[512]{0:T(512)}, u32[]{:S(2)}) copy-start(f32[512]{0:T(512)} %param.30) | copy-start | bytes 6148
Sparse Core Ops, SparseCore 0:
  26.6 56.4 all-reduce.18
  161.3 51.0 all-reduce.20
where the time goes:
time: 255 us; the launch traced here: 254 us
  blocking collectives  123 us (48%)
  waiting for transfers between devices  80.2 us (31%)
  matrix products  22.8 us (9%)
  between operations  15.6 us (6%)
  local copies, waits for them, and re-layouts  7.82 us (3%)
  other arithmetic  3.84 us (2%)
    unnamed x4, waiting for transfers between devices  80.2 us
    unnamed x4, blocking collectives  49.8 us
    psum x1, blocking collectives, local(): own_squares = lax.psum(own_squares, 'tp')  14.6 us
    all_gather x1, blocking collectives, local(): lax.all_gather(activated, 'tp', axis=0, tiled=True)  14.6 us
    all_gather x1, blocking collectives, local(): lax.all_gather(mixed, 'tp', axis=0, tiled=True)  14 us
    psum x1, blocking collectives, local(): middle_squares = lax.psum(middle_squares, 'tp')  13.6 us
    all_gather x1, blocking collectives, local(): lax.all_gather(scaled_in, 'kv', axis=0, tiled=True)  9.66 us
    dot_general x8, matrix products, local(): jnp.dot(rows_part, matrix, preferred_element_type=jnp.float32)  9.1 us
  transfers between devices with their start and end apart: 2, of which 2 were waited for; matrix products, arithmetic and copies ran while one was open for 1% of the time, Pallas kernels for 0%

commit v1 on v0

--- a/solution.py
+++ b/solution.py
@@ -169,7 +169,16 @@
     middle = stream + mixer_out
     scaled_mid = (middle * channel_gain).astype(jnp.bfloat16)
     middle_squares = jnp.sum(middle * middle, axis=1)
-    middle_squares = lax.psum(middle_squares, "tp")
+
+    def time_cards_on(raw, axis_key):
+        n_dev_all = lax.psum(1, axis_name=axis_key)
+        ready = lambda small: [(dev_j, dev_j ^ small) for dev_j in range(n_dev_all)]
+        z2 = raw
+        for src_i in range(n_dev_all.bit_length() - 1):
+            z2 = z2 + lax.ppermute(z2, axis_name=axis_key, perm=ready(1 << src_i))
+        return z2
+
+    middle_squares = time_cards_on(middle_squares, "tp")
     middle_rows, middle_all = (
         lax.all_gather(scaled_mid, "kv", axis=0, tiled=True),
         lax.all_gather(middle_squares.astype(jnp.bfloat16), "kv", axis=0, tiled=True).astype(

time: 255 us -> 240 us (0.941)
  blocking collectives: 123 us -> 110 us
    psum x1 -> x0, blocking collectives: 13.6 us -> none  [local(): middle_squares = lax.psum(middle_squares, 'tp')]
    unnamed x4, waiting for transfers between devices: 80.2 us -> 71.9 us
    ppermute x0 -> x3, waiting for transfers between devices: none -> 7.46 us  [time_cards_on(): z2 = z2 + lax.ppermute(z2, axis_name=axis_key, perm=ready(1 << src_i))]
    unnamed x42 -> x44, local copies, waits for them, and re-layouts: 7.67 us -> 8.45 us
  transfers between devices with their start and end apart: 2 -> 5, of which waited for: 2 -> 4; matrix products, arithmetic and copies ran while one was open for 1% -> 2% of each run, Pallas kernels for 0% -> 0%
where the time goes in v1:
time: 240 us; the launch traced here: 239 us
  blocking collectives  110 us (46%)
  waiting for transfers between devices  79.4 us (33%)
  matrix products  20.9 us (9%)
  between operations  15.6 us (6%)
  local copies, waits for them, and re-layouts  8.6 us (4%)
  other arithmetic  3.85 us (2%)
    unnamed x4, waiting for transfers between devices  71.9 us
    unnamed x4, blocking collectives  49.8 us
    psum x1, blocking collectives, local(): own_squares = lax.psum(own_squares, 'tp')  14.6 us
    all_gather x1, blocking collectives, local(): lax.all_gather(activated, 'tp', axis=0, tiled=True)  14.6 us
    all_gather x1, blocking collectives, local(): lax.all_gather(mixed, 'tp', axis=0, tiled=True)  14 us
    all_gather x1, blocking collectives, local(): lax.all_gather(scaled_in, 'kv', axis=0, tiled=True)  9.66 us
    dot_general x8, matrix products, local(): jnp.dot(rows_part, matrix, preferred_element_type=jnp.float32)  9.1 us
    unnamed x44, local copies, waits for them, and re-layouts  8.45 us
  transfers between devices with their start and end apart: 5, of which 4 were waited for; matrix products, arithmetic and copies ran while one was open for 2% of the time, Pallas kernels for 0%

profile of v1, /device:TPU:0, one launch (start us, length us, event | category | flops | bytes accessed | tf_op | source)
XLA Modules:
  0.0 239.0 jit_solution(1790705692135191120)
XLA Ops:
  7.5 9.7 %all-gather = bf16[4,4,512]{2,1,0:T(4,128)(2,1)S(1)} all-gather(bf16[1,4,512]{2,1,0:T(4,128)(2,1)S(1)} %get-tuple-element.28), channel_id=1, replica_groups=mesh['kv'=4,'tp'=8] {'kv'}, dimensions={0}, use_global_device_ids=true | all-gather | bytes 20480 | tf_op jit(solution)/shard_map/all_gather | solution.py:112
  17.3 2.7 %convolution_convert_fusion.2 = bf16[8,2048]{1,0:T(8,128)(2,1)} fusion(bf16[512,2048]{1,0:T(8,128)(2,1)} %param.21, bf16[8,1,512]{2,0,1:T(8,128)(2,1)S(1)} %copy.26), kind=kOutput, calls=%fused_computation.2 | convolution fusion | flops 16793600 | bytes 2138112 | tf_op jit(solution)/shard_map/dot_general | solution.py:127
  26.7 14.6 %psum.7 = bf16[4]{0:T(256)(128)(2,1)S(1)} all-reduce(f32[4]{0:T(128)S(1)} %get-tuple-element.27), channel_id=1, replica_groups=mesh['kv'=4,'tp'=8] {'tp'}, use_global_device_ids=true, to_apply=%region_1.0 | all-reduce | flops 4 | bytes 24 | tf_op jit(solution)/shard_map/psum | solution.py:110
  43.5 8.9 %all-reduce = bf16[16]{0:T(256)(128)(2,1)S(1)} all-reduce(bf16[16]{0:T(256)(128)(2,1)S(1)} %dynamic-update-slice), channel_id=1, replica_groups=mesh['kv'=4,'tp'=8] {'kv'}, use_global_device_ids=true, to_apply=%add | all-reduce | flops 16 | bytes 64
  54.1 29.0 %all-reduce.19.cloned.1.call-done = (bf16[8,1024]{1,0:T(8,128)(2,1)}, bf16[8,1024]{1,0:T(8,128)(2,1)}, bf16[8,2048]{1,0:T(8,128)(2,1)}, bf16[8,2048]{1,0:T(8,128...) async-done(((bf16[8,1024]{1,0:T(8,128)(2,1)}, bf16[8,1024]{1,0:T(8,128)(2,1)}, ...) | async-done | bytes 196624
  83.0 1.4 dynamic-slice_reduce_fusion.6
  84.5 1.4 dynamic-slice_reduce_fusion.4
  86.3 3.6 %fusion.19 = f32[2,4,1,512]{3,2,1,0:T(1,128)S(1)} fusion(f32[2,4,256,512]{3,2,1,0:T(8,128)} %param.24, bf16[2,4,256,1]{2,1,0,3:T(4,128)(2,1)S(1)} %fusion.30), kind=kOutput, calls=%fused_computation.53 | convolution fusion | flops 12582912 | bytes 4214784 | tf_op jit(solution)/shard_map/shk,shkv->shv/dot_general | solution.py:70
  89.9 1.5 dynamic-slice_reduce_fusion
  91.6 1.5 fusion.27
  93.4 1.5 dynamic-slice_reduce_fusion.2
  95.1 14.0 %all-gather.1 = bf16[8,2,2048]{2,1,0:T(2,128)(2,1)S(1)} all-gather(bf16[1,2,2048]{2,1,0:T(2,128)(2,1)S(1)} %reshape.210), channel_id=1, replica_groups=mesh['kv'=4,'tp'=8] {'tp'}, dimensions={0}, use_global_device_ids=true | all-gather | bytes 73728 | tf_op jit(solution)/shard_map/all_gather | solution.py:162
  109.1 2.0 convolution_convert_fusion.7
  111.0 16.0 %all-reduce.10 = bf16[16,512]{1,0:T(8,128)(2,1)S(1)} all-reduce(bf16[16,512]{1,0:T(8,128)(2,1)S(1)} %convolution_convert_fusion.7), channel_id=10, replica_groups=mesh['kv'=4,'tp'=8] {'kv'}, use_global_device_ids=true, to_apply=%region_13.14.clone | all-reduce | flops 8192 | bytes 32768
  127.2 7.2 %all-gather.2 = bf16[4,4,512]{2,1,0:T(4,128)(2,1)S(1)} all-gather(bf16[1,4,512]{2,1,0:T(4,128)(2,1)S(1)} %get-tuple-element.20), channel_id=1, replica_groups=mesh['kv'=4,'tp'=8] {'kv'}, dimensions={0}, use_global_device_ids=true | all-gather | bytes 20480 | tf_op jit(solution)/shard_map/all_gather | solution.py:183
  134.5 1.1 convolution_convert_fusion
  136.3 1.1 convolution_convert_fusion.1
  137.5 3.6 %collective-permute-done.1 = f32[4]{0:T(128)S(1)} collective-permute-done((f32[4]{0:T(128)S(1)}, f32[4]{0:T(128)S(1)}, u32[]{:S(2)}, u32[]{:S(2)}) %collective-permute-start.1) | collective-permute-done | bytes 48 | tf_op jit(solution)/shard_map/ppermute | solution.py:178
  141.6 3.9 %collective-permute-done.2 = f32[4]{0:T(128)S(1)} collective-permute-done((f32[4]{0:T(128)S(1)}, f32[4]{0:T(128)S(1)}, u32[]{:S(2)}, u32[]{:S(2)}) %collective-permute-start.2) | collective-permute-done | bytes 48 | tf_op jit(solution)/shard_map/ppermute | solution.py:178
  145.8 8.9 %all-reduce.1 = bf16[16]{0:T(256)(128)(2,1)S(1)} all-reduce(bf16[16]{0:T(256)(128)(2,1)S(1)} %dynamic-update-slice.1), channel_id=1, replica_groups=mesh['kv'=4,'tp'=8] {'kv'}, use_global_device_ids=true, to_apply=%add.1 | all-reduce | flops 16 | bytes 64
  154.8 42.9 %all-reduce.21.cloned.1.call-done = (bf16[16,2816]{1,0:T(8,128)(2,1)}, bf16[16,2816]{1,0:T(8,128)(2,1)}) async-done(((bf16[16,2816]{1,0:T(8,128)(2,1)}, bf16[16,2816]{1,0:T(8,128)(2,1)}), (bf16[16,2816]{1,0:T(8,128)(2,1)}, bf16[16,2816]{1,0:T(8,128)(2,1)})) %all-reduce.21.cloned.1.call-update) | async-done | bytes 180240
  198.6 14.6 %all-gather.3 = bf16[8,2,2816]{2,1,0:T(2,128)(2,1)S(1)} all-gather(bf16[1,2,2816]{2,1,0:T(2,128)(2,1)S(1)} %fusion.6), channel_id=1, replica_groups=mesh['kv'=4,'tp'=8] {'tp'}, dimensions={0}, use_global_device_ids=true | all-gather | bytes 101376 | tf_op jit(solution)/shard_map/all_gather | solution.py:206
  213.2 2.3 convolution_convert_fusion.6
  215.5 16.0 %all-reduce.13 = bf16[16,512]{1,0:T(8,128)(2,1)S(1)} all-reduce(bf16[16,512]{1,0:T(8,128)(2,1)S(1)} %convolution_convert_fusion.6), channel_id=13, replica_groups=mesh['kv'=4,'tp'=8] {'kv'}, use_global_device_ids=true, to_apply=%region_17.18.clone | all-reduce | flops 8192 | bytes 32768
  (95 shorter events, 14.0 us)
Async XLA Ops:
  6.5 128.0 %copy-start = (bf16[512,2816]{1,0:T(8,128)(2,1)S(1)}, bf16[512,2816]{1,0:T(8,128)(2,1)}, u32[]{:S(2)}) copy-start(bf16[512,2816]{1,0:T(8,128)(2,1)} %param.32) | copy-start | bytes 8650756
  6.5 76.5 %all-reduce.19.cloned.1.call-start = ((), (), s32[]{:S(2)}) async-start(), calls=%async_computation | async-start | bytes 393216
  17.2 2.8 %copy-start.1 = (bf16[512,2048]{1,0:T(8,128)(2,1)S(1)}, bf16[512,2048]{1,0:T(8,128)(2,1)}, u32[]{:S(2)}) copy-start(bf16[512,2048]{1,0:T(8,128)(2,1)} %param.21) | copy-start | bytes 6291460
  17.3 3.7 %copy-start.2 = (bf16[512,2048]{1,0:T(8,128)(2,1)S(1)}, bf16[512,2048]{1,0:T(8,128)(2,1)}, u32[]{:S(2)}) copy-start(bf16[512,2048]{1,0:T(8,128)(2,1)} %param.22) | copy-start | bytes 6291460
  21.0 2.0 copy-start.3
  22.0 2.7 %copy-start.4 = (bf16[512,1024]{1,0:T(8,128)(2,1)S(1)}, bf16[512,1024]{1,0:T(8,128)(2,1)}, u32[]{:S(2)}) copy-start(bf16[512,1024]{1,0:T(8,128)(2,1)} %param.20) | copy-start | bytes 3145732
  23.0 3.5 %copy-start.11 = (s32[2]{0:T(128)S(1)}, s32[2]{0:T(128)}, u32[]{:S(2)}) copy-start(s32[2]{0:T(128)} %param.27) | copy-start | bytes 28
  23.0 18.3 %copy-start.13 = (u32[32]{0:T(128)S(1)}, u32[32]{0:T(128)}, u32[]{:S(2)}) copy-start(u32[32]{0:T(128)} %constant.69) | copy-start | bytes 388
  23.0 18.9 %copy-start.10 = (u32[32]{0:T(128)S(1)}, u32[32]{0:T(128)}, u32[]{:S(2)}) copy-start(u32[32]{0:T(128)} %constant.57) | copy-start | bytes 388
  23.0 29.5 %copy-start.12 = (f32[4]{0:T(128)S(1)}, f32[4]{0:T(128)}, u32[]{:S(2)}) copy-start(f32[4]{0:T(128)} %param.23) | copy-start | bytes 52
  23.0 29.5 %copy-start.8 = (f32[2048]{0:T(1024)S(1)}, f32[2048]{0:T(1024)}, u32[]{:S(2)}) copy-start(f32[2048]{0:T(1024)} %param.28) | copy-start | bytes 24580
  23.9 62.2 %copy-start.6 = (bf16[2,4,128,256]{3,2,1,0:T(8,128)(2,1)S(1)}, bf16[2,4,128,256]{3,2,1,0:T(8,128)(2,1)}, u32[]{:S(2)}) copy-start(bf16[2,4,128,256]{3,2,1,0:T(8,128)(2,1)} %param.25) | copy-start | bytes 1572868
  26.4 171.3 %all-reduce.21.cloned.1.call-start = ((), (), s32[]{:S(2)}) async-start(), calls=%async_computation.1 | async-start | bytes 360448
  89.9 37.1 %copy-start.7 = (bf16[4,512]{1,0:T(4,128)(2,1)S(1)}, bf16[4,512]{1,0:T(4,128)(2,1)}, u32[]{:S(2)}) copy-start(bf16[4,512]{1,0:T(4,128)(2,1)} %param.17) | copy-start | bytes 12292
  89.9 37.1 %copy-start.9 = (f32[512]{0:T(512)S(1)}, f32[512]{0:T(512)}, u32[]{:S(2)}) copy-start(f32[512]{0:T(512)} %param.30) | copy-start | bytes 6148
  127.2 10.3 %collective-permute-start = (f32[4]{0:T(128)S(1)}, f32[4]{0:T(128)S(1)}, u32[]{:S(2)}, u32[]{:S(2)}) collective-permute-start(f32[4]{0:T(128)S(1)} %get-tuple-element.19), channel_id=1, source_target_pairs={{0,1},{1,0},{2,3},{3,2},{4,5},{5,4},{6,7},{7,6},{8,9},{9,8},{10,11... | collective-permute-start | bytes 56 | tf_op jit(solution)/shard_map/ppermute | solution.py:178
  134.5 1.9 copy-start.5
  137.5 3.6 %collective-permute-start.1 = (f32[4]{0:T(128)S(1)}, f32[4]{0:T(128)S(1)}, u32[]{:S(2)}, u32[]{:S(2)}) collective-permute-start(f32[4]{0:T(128)S(1)} %add.101), channel_id=1, source_target_pairs={{0,2},{1,3},{2,0},{3,1},{4,6},{5,7},{6,4},{7,5},{8,10},{9,11},{10,... | collective-permute-start | bytes 56 | tf_op jit(solution)/shard_map/ppermute | solution.py:178
  141.1 4.5 %collective-permute-start.2 = (f32[4]{0:T(128)S(1)}, f32[4]{0:T(128)S(1)}, u32[]{:S(2)}, u32[]{:S(2)}) collective-permute-start(f32[4]{0:T(128)S(1)} %add.102), channel_id=1, source_target_pairs={{0,4},{1,5},{2,6},{3,7},{4,0},{5,1},{6,2},{7,3},{8,12},{9,13},{10,... | collective-permute-start | bytes 56 | tf_op jit(solution)/shard_map/ppermute | solution.py:178
Sparse Core Ops, SparseCore 0:
  26.6 56.4 all-reduce.18
  145.9 51.7 all-reduce.20
